TPU v7x, 32 devices: a whole 2x2x4 slice. The times are simulated.
32 devices in a mesh: fs: 8 (over z, y), tp: 4 (over x, core).
Axes of the slice: x: 2, y: 2, z: 4, core: 2. Of those that a mesh axis runs over, the one named last changes fastest.
Arguments:
- tokens: bfloat16 [8192, 2048], P('fs'), may hold values from -6 to 6
- norm_gain: float32 [2048], replicated, may hold values from 0.1 to 1.9
- gate_weight: bfloat16 [2048, 4096], P('fs', 'tp'), may hold values from -0.125 to 0.125
- up_weight: bfloat16 [2048, 4096], P('fs', 'tp'), may hold values from -0.125 to 0.125
- down_weight: bfloat16 [4096, 2048], P('tp', 'fs'), may hold values from -2 to 2
- out_gain: float32 [2048], P('tp'), may hold values from 0.1 to 1.9
Outputs:
- result: bfloat16 [8192, 2048], P('fs', 'tp')
All inputs are finite; a program needn't handle non-finite values.
Results may differ from a plain program's by a relative error of at most 0.014.
Values may be sent and summed in bfloat16 or wider, within the bound.
A program may use at most 64 MiB of HBM per device.

v0:
```python
import jax
import jax.numpy as jnp
from jax import lax
from jax.sharding import PartitionSpec as P

EPSILON = 1e-06


def body(tokens, norm_gain, gate_weight, up_weight, down_weight, out_gain):
    values = tokens.astype(jnp.float32)
    normed = (
        values * lax.rsqrt(jnp.mean(values * values, axis=1, keepdims=True) + EPSILON) * norm_gain
    ).astype(jnp.bfloat16)
    gate_all, up_all = (
        lax.all_gather(gate_weight, "fs", axis=0, tiled=True),
        lax.all_gather(up_weight, "fs", axis=0, tiled=True),
    )
    gate_proj = jnp.dot(normed, gate_all, preferred_element_type=jnp.float32)
    up_proj = jnp.dot(normed, up_all, preferred_element_type=jnp.float32)
    hidden = (jax.nn.silu(gate_proj) * up_proj).astype(jnp.bfloat16)
    partial_value = jnp.dot(
        hidden,
        lax.all_gather(down_weight, "fs", axis=1, tiled=True),
        preferred_element_type=jnp.float32,
    )
    own_width = out_gain.shape[0]
    own_columns = lax.psum_scatter(
        partial_value.astype(jnp.bfloat16), "tp", scatter_dimension=1, tiled=True
    ).astype(jnp.float32)
    squares = lax.psum(jnp.sum(own_columns * own_columns, axis=1), "tp")
    mean_square = squares / (own_width * lax.axis_size("tp"))
    scaled = own_columns * lax.rsqrt(mean_square + EPSILON)[:, None] * out_gain[None, :]
    return scaled.astype(jnp.bfloat16)


def solution(mesh):
    return jax.shard_map(
        body,
        mesh=mesh,
        in_specs=(P("fs", None), P(), P("fs", "tp"), P("fs", "tp"), P("tp", "fs"), P("tp")),
        out_specs=P("fs", "tp"),
        check_vma=False,
    )
```

profile of v0, /device:TPU:0, one launch (start us, length us, event | category | flops | bytes accessed | tf_op | source)
XLA Modules:
  0.0 308.2 jit_solution(11775894596299125198)
XLA Ops:
  6.5 0.0 copy-start.1
  6.5 0.0 all-gather.4.cloned.1.call-start
  6.5 0.7 all-gather.4.cloned.1.call-update
  7.3 0.0 all-gather.6.cloned.1.call-start
  7.3 0.7 all-gather.6.cloned.1.call-update
  8.0 0.0 all-gather.8.cloned.1.call-start
  8.1 0.7 all-gather.8.cloned.1.call-update
  8.7 0.0 reduce-scatter.2.cloned.1.call-start
  8.8 3.1 fusion
  11.9 73.1 %all-gather.4.cloned.1.call-done = bf16[2048,1024]{1,0:T(8,128)(2,1)} async-done(((bf16[256,1024]{1,0:T(8,128)(2,1)}), bf16[2048,1024]{1,0:T(8,128)(2,1)}) %all-gather.4.cloned.1.call-update) | async-done | bytes 4194320 | tf_op jit(solution)/shard_map/all_gather | solution.py:15
  85.0 0.0 copy-done.1
  85.0 10.0 %fusion.7 = f32[1024,1024]{1,0:T(8,128)} fusion(bf16[2048,1024]{1,0:T(8,128)(2,1)} %all-gather.4.cloned.1.call-done, bf16[1024,2048]{1,0:T(8,128)(2,1)} %param.6, f32[2048]{0:T(1024)S(1)} %copy-done.1, f32[1024]{0:T(1024)S(1)} %add_rsqrt_fusion.1), kind=kOutput, calls=%fused_computation.12 | convolution fusion | flops 4303355904 | bytes 12595200 | tf_op jit(solution)/shard_map/dot_general | solution.py:18
  95.0 63.5 %all-gather.6.cloned.1.call-done = bf16[2048,1024]{1,0:T(8,128)(2,1)} async-done(((bf16[256,1024]{1,0:T(8,128)(2,1)}), bf16[2048,1024]{1,0:T(8,128)(2,1)}) %all-gather.6.cloned.1.call-update) | async-done | bytes 4194320 | tf_op jit(solution)/shard_map/all_gather | solution.py:16
  158.5 75.3 %all-gather.8.cloned.1.call-done = bf16[1024,2048]{1,0:T(8,128)(2,1)} async-done(((bf16[1024,256]{1,0:T(8,128)(2,1)}), bf16[1024,2048]{1,0:T(8,128)(2,1)}) %all-gather.8.cloned.1.call-update) | async-done | bytes 4194320 | tf_op jit(solution)/shard_map/all_gather | solution.py:23
  233.7 15.3 %convolution_convert_fusion = bf16[1024,2048]{1,0:T(8,128)(2,1)} fusion(bf16[1024,2048]{1,0:T(8,128)(2,1)} %all-gather.8.cloned.1.call-done, f32[1024,1024]{1,0:T(8,128)} %fusion.7, bf16[2048,1024]{1,0:T(8,128)(2,1)} %all-gather.6.cloned.1.call-done, bf16[1024,2048]{1,0:T(8,128)(2,1)} %param.6, f32[2048]{0:T(1024)S(1)} %copy-done.1, ...), kind=kOutput, calls=%fused_computation.6 | convolution fusion | flops 8606711808 | bytes 20983808 | tf_op jit(solution)/shard_map/dot_general | solution.py:21
  249.1 0.0 copy-start
  249.1 0.0 reduce-scatter.2.cloned.1.call-update
  249.1 42.7 %reduce-scatter.2.cloned.1.call-done = bf16[1024,512]{1,0:T(8,128)(2,1)} async-done(((bf16[1024,2048]{1,0:T(8,128)(2,1)}), bf16[1024,512]{1,0:T(8,128)(2,1)}) %reduce-scatter.2.cloned.1.call-update) | async-done | bytes 1048592 | tf_op jit(solution)/shard_map/reduce_scatter | solution.py:27
  291.9 1.5 fusion.3
  293.4 5.8 %psum.7 = f32[1024]{0:T(1024)S(1)} all-reduce(f32[1024]{0:T(1024)S(1)} %fusion.3), channel_id=1, replica_groups=mesh['fs'=8,'tp'=4] {'tp'}, use_global_device_ids=true, to_apply=%region_3.4 | all-reduce | flops 1024 | bytes 8192 | tf_op jit(solution)/shard_map/psum | solution.py:30
  299.1 0.0 copy-done
  299.1 2.5 fusion.5
  (2 shorter events, 0.0 us)
Async XLA Ops:
  6.5 78.5 %copy-start.1 = (f32[2048]{0:T(1024)S(1)}, f32[2048]{0:T(1024)}, u32[]{:S(2)}) copy-start(f32[2048]{0:T(1024)} %param.7) | copy-start | bytes 24580
  6.5 78.5 %all-gather.4.cloned.1.call-start = ((), (), s32[]{:S(2)}) async-start(), calls=%async_computation.1 | async-start | bytes 4718592 | tf_op jit(solution)/shard_map/all_gather | solution.py:15
  7.3 151.2 %all-gather.6.cloned.1.call-start = ((), (), s32[]{:S(2)}) async-start(), calls=%async_computation.2 | async-start | bytes 4718592 | tf_op jit(solution)/shard_map/all_gather | solution.py:16
  8.0 225.7 %all-gather.8.cloned.1.call-start = ((), (), s32[]{:S(2)}) async-start(), calls=%async_computation.3 | async-start | bytes 4718592 | tf_op jit(solution)/shard_map/all_gather | solution.py:23
  8.7 283.1 %reduce-scatter.2.cloned.1.call-start = ((), (), s32[]{:S(2)}) async-start(), calls=%async_computation.4 | async-start | bytes 5242880 | tf_op jit(solution)/shard_map/reduce_scatter | solution.py:27
  249.1 50.0 %copy-start = (f32[512]{0:T(512)S(1)}, f32[512]{0:T(512)}, u32[]{:S(2)}) copy-start(f32[512]{0:T(512)} %param.11) | copy-start | bytes 6148
Sparse Core Ops, SparseCore 0:
  9.5 75.5 all-gather.3
  87.1 71.3 all-gather.5
  160.5 73.1 all-gather.7
  249.2 42.5 reduce-scatter.1
where the time goes:
time: 308 us
  waiting for transfers between devices  257 us (83%)
  matrix products  25.3 us (8%)
  between operations  13.1 us (4%)
  other arithmetic  7.09 us (2%)
  blocking collectives  5.77 us (2%)
    all_gather x1, waiting for transfers between devices, body(): lax.all_gather(down_weight, 'fs', axis=1, tiled=True)  75.3 us
    all_gather x1, waiting for transfers between devices, body(): lax.all_gather(gate_weight, 'fs', axis=0, tiled=True)  73.1 us
    all_gather x1, waiting for transfers between devices, body(): lax.all_gather(up_weight, 'fs', axis=0, tiled=True)  63.5 us
    reduce_scatter x1, waiting for transfers between devices, body(): lax.psum_scatter(partial_value.astype(jnp.bfloat16), 'tp', scatter_dimens...  42.7 us
    dot_general x1, matrix products, body(): jnp.dot(hidden, lax.all_gather(down_weight, 'fs', axis=1, tiled=True), pr...  15.3 us
    dot_general x1, matrix products, body(): gate_proj = jnp.dot(normed, gate_all, preferred_element_type=jnp.float32)  9.96 us
  transfers between devices with their start and end apart: 4, of which 4 were waited for; matrix products, arithmetic and copies ran while one was open for 4% of the time, Pallas kernels for 0%

commit v1 on v0

v1 whole, which is shorter than its diff:
```python
import functools

import jax
import jax.numpy as jnp
from jax import lax
from jax.experimental import pallas as pl
from jax.experimental.pallas import tpu as pltpu
from jax.sharding import PartitionSpec as P

EPSILON = 1e-06
MESH = pl.DeviceIdType.MESH
PIECES = 4
COLUMN_TILE = 256


def ring_layout(n, n_tp):
    ny = max(n_tp // 2, 1)
    if n % ny or (n // ny) % 2:
        ny = 1
    nz, rest = n // ny, max(ny - 1, 1)

    def position(fs):
        z, y = fs // ny, fs % ny
        k = nz - 1 - z
        odd = k % 2
        back = nz + k * rest + (1 - odd) * (y - 1) + odd * (ny - 1 - y)
        return jnp.where(y == 0, z, back)

    def index(pos):
        q = jnp.maximum(pos - nz, 0)
        k, r = q // rest, q % rest
        odd = k % 2
        back = (nz - 1 - k) * ny + (1 - odd) * (1 + r) + odd * (ny - 1 - r)
        return jnp.where(pos < nz, pos * ny, back)

    return position, index


def kernel(
    n, n_tp, tokens_hbm, norm_gain, gate_hbm, up_hbm, down_hbm, out_gain, out_ref,
    tok, normed, gate, up, down, gate_acc, up_acc, hidden, parts, sib, far, own, sq, sq_all,
    local_sem, ring_send, ring_recv, sib_send, sib_recv, far_send, far_recv, sq_send, sq_recv,
):
    half = n // 2
    nx, nb = n_tp // 2, n // n_tp
    n_tok, d_model = tok.shape
    rows_in = gate.shape[1]
    n_hid, width = down.shape[1], down.shape[2]
    piece = n_tok // PIECES
    position, index = ring_layout(n, n_tp)
    fs, tp = lax.axis_index("fs"), lax.axis_index("tp")
    x, core = tp // 2, tp % 2
    me = position(fs)
    block_of = {}
    for h in range(half + 1):
        block_of[0, h] = index((me + n - h) % n)
        block_of[1, h] = index((me + h) % n)
    target = (block_of[1, 1], block_of[0, 1])
    sibling = x * 2 + 1 - core

    barrier = pltpu.get_barrier_semaphore()
    for fs_id in target:
        pl.semaphore_signal(barrier, inc=1, device_id={"fs": fs_id}, device_id_type=MESH)
    for d in range(1, n_tp):
        pl.semaphore_signal(
            barrier, inc=1, device_id={"tp": (tp + d) % n_tp}, device_id_type=MESH
        )
    loads = [
        pltpu.make_async_copy(tokens_hbm, tok, local_sem.at[0]),
        pltpu.make_async_copy(gate_hbm, gate.at[fs], local_sem.at[1]),
        pltpu.make_async_copy(up_hbm, up.at[fs], local_sem.at[2]),
        pltpu.make_async_copy(down_hbm, down.at[fs], local_sem.at[3]),
    ]
    for load in loads:
        load.start()
    pl.semaphore_wait(barrier, 2 + n_tp - 1)

    def view(c, b, h, way):
        if c < 2:
            ref = (gate, up)[c]
            if h == half:
                return ref.at[b, pl.ds(way * (rows_in // 2), rows_in // 2)]
            return ref.at[b]
        return down.at[b, pl.ds((c - 2) * (n_hid // 2), n_hid // 2)]

    def ring_copy(c, way, h, b, first=False):
        dst = view(c, b, h, way)
        src = (gate_hbm, up_hbm)[c] if first and c < 2 else dst
        return pltpu.make_async_remote_copy(
            src_ref=src,
            dst_ref=dst,
            send_sem=ring_send.at[way, h - 1, c],
            recv_sem=ring_recv.at[way, h - 1, c],
            device_id={"fs": target[way]},
            device_id_type=MESH,
        )

    sends = []

    def send(c, way, h):
        copy = ring_copy(c, way, h, block_of[way, h - 1], h == 1)
        copy.start()
        sends.append(copy)

    def arrive(c, way, h):
        ring_copy(c, way, h, block_of[way, h]).wait_recv()

    for c in (0, 1):
        for way in (0, 1):
            send(c, way, 1)

    loads[0].wait()
    tile = min(128, n_tok)

    @pl.loop(0, n_tok // tile)
    def _(i):
        rows = pl.ds(pl.multiple_of(i * tile, tile), tile)
        v = tok[rows, :].astype(jnp.float32)
        r = lax.rsqrt(jnp.mean(v * v, axis=1, keepdims=True) + EPSILON)
        out = (v * r * norm_gain[...]).astype(jnp.bfloat16)
        for j in range(n):
            normed[j, rows, :] = out[:, j * rows_in:(j + 1) * rows_in]

    def accumulate(b, mode):
        n_col = gate.shape[2]
        step = min(COLUMN_TILE, n_col)

        @pl.loop(0, n_col // step)
        def _(i):
            cols = pl.ds(pl.multiple_of(i * step, step), step)
            a = normed[b]
            g = jnp.dot(a, gate[b, :, cols], preferred_element_type=jnp.float32)
            u = jnp.dot(a, up[b, :, cols], preferred_element_type=jnp.float32)
            if mode != "first":
                g = g + gate_acc[:, cols]
                u = u + up_acc[:, cols]
            if mode == "last":
                hidden[:, cols] = (g * (1.0 / (1.0 + jnp.exp(-g))) * u).astype(jnp.bfloat16)
            else:
                gate_acc[:, cols] = g
                up_acc[:, cols] = u

    loads[1].wait()
    loads[2].wait()
    accumulate(fs, "first")
    loads[3].wait()

    for h in range(1, half + 1):
        for c in (0, 1):
            for way in (0, 1):
                arrive(c, way, h)
                if h < half:
                    send(c, way, h + 1)
        if h == half - 1:
            for c in (2, 3):
                for way in (0, 1):
                    send(c, way, 1)
        if h < half:
            accumulate(block_of[0, h], "mid")
            accumulate(block_of[1, h], "mid")
        else:
            accumulate(block_of[0, h], "last")

    def owner(b):
        t = b // nb
        return t // 2, t % 2, b % nb

    def piece_rows(q):
        return pl.ds(pl.multiple_of(q * piece, piece), piece)

    def sib_copy(b, slot, q):
        return pltpu.make_async_remote_copy(
            src_ref=parts.at[b, piece_rows(q)],
            dst_ref=sib.at[slot, piece_rows(q)],
            send_sem=sib_send.at[slot, q],
            recv_sem=sib_recv.at[slot, q],
            device_id={"tp": sibling},
            device_id_type=MESH,
        )

    def far_copy(b, x_to, x_from, k, q):
        return pltpu.make_async_remote_copy(
            src_ref=parts.at[b, piece_rows(q)],
            dst_ref=far.at[x_from, k, piece_rows(q)],
            send_sem=far_send.at[x_to * nb + k, q],
            recv_sem=far_recv.at[x_from, k, q],
            device_id={"tp": x_to * 2 + core},
            device_id_type=MESH,
        )

    def multiply(b):
        x_to, core_to, k = owner(b)

        @pl.loop(0, PIECES)
        def _(q):
            rows = piece_rows(q)
            parts[b, rows, :] = jnp.dot(
                hidden[rows, :], down[b], preferred_element_type=jnp.float32
            ).astype(jnp.bfloat16)

            @pl.when(core_to != core)
            def _():
                sib_copy(b, x_to * nb + k, q).start()

    def reduce(b):
        x_to, core_to, k = owner(b)

        @pl.when((core_to == core) & (x_to != x))
        def _():
            @pl.loop(0, PIECES)
            def _(q):
                rows = piece_rows(q)
                slot = x_to * nb + k
                sib_copy(b, slot, q).wait_recv()
                parts[b, rows, :] = (
                    parts[b, rows, :].astype(jnp.float32) + sib[slot, rows, :].astype(jnp.float32)
                ).astype(jnp.bfloat16)
                far_copy(b, x_to, x, k, q).start()

    multiply(fs)
    pending = [fs]
    for h in range(1, half + 1):
        for c in (2, 3):
            for way in (0, 1):
                if h < half or way == c - 2:
                    arrive(c, way, h)
                if h < half - 1 or (h == half - 1 and way == c - 2):
                    send(c, way, h + 1)
            if c == 2:
                for b in pending:
                    reduce(b)
                pending = []
        for way in (0, 1) if h < half else (0,):
            multiply(block_of[way, h])
            pending.append(block_of[way, h])
    for b in pending:
        reduce(b)

    @pl.loop(0, PIECES)
    def _(q):
        rows = piece_rows(q)
        squares = jnp.zeros((piece, 1), jnp.float32)
        for k in range(nb):
            b, slot = tp * nb + k, x * nb + k
            v = parts[b, rows, :].astype(jnp.float32)
            sib_copy(b, slot, q).wait_recv()
            v = v + sib[slot, rows, :].astype(jnp.float32)
            for d in range(1, nx):
                x_from = (x + d) % nx
                far_copy(b, x, x_from, k, q).wait_recv()
                v = v + far[x_from, k, rows, :].astype(jnp.float32)
            own[k, rows, :] = v
            squares = squares + jnp.sum(v * v, axis=1, keepdims=True)
        sq[q] = jnp.transpose(jnp.broadcast_to(squares, (piece, 128)))[0:8, :]

    def sq_copy(to, slot):
        return pltpu.make_async_remote_copy(
            src_ref=sq,
            dst_ref=sq_all.at[slot],
            send_sem=sq_send.at[to],
            recv_sem=sq_recv.at[slot],
            device_id={"tp": to},
            device_id_type=MESH,
        )

    others = [(tp + d) % n_tp for d in range(1, n_tp)]
    for t in others:
        sq_copy(t, tp).start()
    for t in others:
        sq_copy(t, t).wait_recv()

    @pl.loop(0, PIECES)
    def _(q):
        rows = piece_rows(q)
        total = sq[q]
        for t in others:
            total = total + sq_all[t, q]
        r = lax.rsqrt(total / d_model + EPSILON)
        r = jnp.transpose(jnp.broadcast_to(r[0:1, :], (128, piece)))[:, 0:1]
        for k in range(nb):
            cols = slice(k * width, (k + 1) * width)
            out_ref[rows, cols] = (own[k, rows, :] * r * out_gain[:, cols]).astype(jnp.bfloat16)

    for t in others:
        sq_copy(t, tp).wait_send()
    for copy in sends:
        copy.wait_send()

    @pl.loop(0, PIECES)
    def _(q):
        for slot in range(nx * nb):
            sib_copy(slot, slot, q).wait_send()
        for d in range(1, nx):
            for k in range(nb):
                far_copy(k, (x + d) % nx, x, k, q).wait_send()


def body(n, n_tp, tokens, norm_gain, gate_weight, up_weight, down_weight, out_gain):
    n_tok, d_model = tokens.shape
    rows_in, n_hid = gate_weight.shape
    width = down_weight.shape[1]
    half, nx, nb = n // 2, n_tp // 2, n // n_tp
    piece = n_tok // PIECES
    bf16, f32 = jnp.bfloat16, jnp.float32
    dma = pltpu.SemaphoreType.DMA
    hbm = pl.BlockSpec(memory_space=pl.ANY)
    vmem = pl.BlockSpec(memory_space=pltpu.VMEM)
    return pl.pallas_call(
        functools.partial(kernel, n, n_tp),
        out_shape=jax.ShapeDtypeStruct((n_tok, out_gain.shape[0]), bf16),
        in_specs=[hbm, vmem, hbm, hbm, hbm, vmem],
        out_specs=vmem,
        scratch_shapes=[
            pltpu.VMEM((n_tok, d_model), bf16),
            pltpu.VMEM((n, n_tok, rows_in), bf16),
            pltpu.VMEM((n, rows_in, n_hid), bf16),
            pltpu.VMEM((n, rows_in, n_hid), bf16),
            pltpu.VMEM((n, n_hid, width), bf16),
            pltpu.VMEM((n_tok, n_hid), f32),
            pltpu.VMEM((n_tok, n_hid), f32),
            pltpu.VMEM((n_tok, n_hid), bf16),
            pltpu.VMEM((n, n_tok, width), bf16),
            pltpu.VMEM((nx * nb, n_tok, width), bf16),
            pltpu.VMEM((nx, nb, n_tok, width), bf16),
            pltpu.VMEM((nb, n_tok, width), f32),
            pltpu.VMEM((PIECES, 8, piece), f32),
            pltpu.VMEM((n_tp, PIECES, 8, piece), f32),
            dma((4,)),
            dma((2, half, 4)),
            dma((2, half, 4)),
            dma((nx * nb, PIECES)),
            dma((nx * nb, PIECES)),
            dma((nx * nb, PIECES)),
            dma((nx, nb, PIECES)),
            dma((n_tp,)),
            dma((n_tp,)),
        ],
        compiler_params=pltpu.CompilerParams(
            collective_id=0, has_side_effects=True, vmem_limit_bytes=62 * 1024 * 1024
        ),
        name="ffn_ring",
    )(tokens, norm_gain[None, :], gate_weight, up_weight, down_weight, out_gain[None, :])


def solution(mesh):
    return jax.shard_map(
        functools.partial(body, mesh.shape["fs"], mesh.shape["tp"]),
        mesh=mesh,
        in_specs=(P("fs", None), P(), P("fs", "tp"), P("fs", "tp"), P("tp", "fs"), P("tp")),
        out_specs=P("fs", "tp"),
        check_vma=False,
    )
```

time: 308 us -> 151 us (0.49)
  waiting for transfers between devices: 257 us -> 0 us
  Pallas kernels: 0 us -> 149 us
  matrix products: 25.3 us -> 0 us
  between operations: 13.1 us -> 0.01 us
  other arithmetic: 7.09 us -> 0 us
  blocking collectives: 5.77 us -> 0 us
    all_gather x3 -> x0, waiting for transfers between devices: 212 us -> none  [the longest x1 75.3 us: body(): lax.all_gather(down_weight, 'fs', axis=1, tiled=True)]
    pallas_call x0 -> x1, Pallas kernels: none -> 149 us  [body(): pl.pallas_call(functools.partial(kernel, n, n_tp), out_shape=jax.ShapeDty...]
    reduce_scatter x1 -> x0, waiting for transfers between devices: 42.7 us -> none  [body(): lax.psum_scatter(partial_value.astype(jnp.bfloat16), 'tp', scatter_dimens...]
    dot_general x2 -> x0, matrix products: 25.3 us -> none  [the longest x1 15.3 us: body(): jnp.dot(hidden, lax.all_gather(down_weight, 'fs', axis=1, tiled=True), pr...]
    psum x1 -> x0, blocking collectives: 5.77 us -> none  [body(): squares = lax.psum(jnp.sum(own_columns * own_columns, axis=1), 'tp')]
    reduce_sum x2 -> x0, other arithmetic: 4.57 us -> none  [the longest x1 3.07 us: body(): jnp.mean(values * values, axis=1, keepdims=True) + EPSILON]
  transfers between devices with their start and end apart: 4 -> 0, of which waited for: 4 -> 0; matrix products, arithmetic and copies ran while one was open for 4% -> 0% of each run, Pallas kernels for 0% -> 0%
where the time goes in v1:
time: 151 us
  Pallas kernels  149 us (99%)
  local copies, waits for them, and re-layouts  2.26 us (1%)
    pallas_call x1, Pallas kernels, body(): pl.pallas_call(functools.partial(kernel, n, n_tp), out_shape=jax.ShapeDty...  149 us

profile of v1, /device:TPU:0, one launch (start us, length us, event | category | flops | bytes accessed | tf_op | source)
XLA Modules:
  0.0 150.8 jit_solution(3458740386059694297)
XLA Ops:
  0.0 148.5 %ffn_ring.1 = bf16[1024,512]{1,0:T(8,128)(2,1)} custom-call(bf16[1024,2048]{1,0:T(8,128)(2,1)} %tokens_hbm.1, f32[1,2048]{1,0:T(1,128)} %bitcast.2, bf16[256,1024]{1,0:T(8,128)(2,1)} %gate_hbm.1, bf16[256,1024]{1,0:T(8,128)(2,1)} %up_hbm.1, bf16[1024,256]{1,0:T(8,128)(2,1)} %down_hbm.1, f32[1,512]{1,0:T(1,128)} %bitcast.3), custom_call_target="tpu_custom_call" | custom-call | tf_op jit(solution)/shard_map/ffn_ring/pallas_call | solution.py:308
  148.6 2.3 %copy.8 = bf16[1024,512]{1,0:T(8,128)(2,1)} copy(bf16[1024,512]{1,0:T(8,128)(2,1)} %ffn_ring.1) | data formatting | bytes 2097152

commit v2 on v1

--- a/solution.py
+++ b/solution.py
@@ -9,7 +9,7 @@
 
 EPSILON = 1e-06
 MESH = pl.DeviceIdType.MESH
-PIECES = 4
+PIECES = 2
 COLUMN_TILE = 256
 
 
@@ -42,7 +42,8 @@
     local_sem, ring_send, ring_recv, sib_send, sib_recv, far_send, far_recv, sq_send, sq_recv,
 ):
     half = n // 2
-    nx, nb = n_tp // 2, n // n_tp
+    nx, cuts = n_tp // 2, down.shape[0] // n
+    nb = n * cuts // n_tp
     n_tok, d_model = tok.shape
     rows_in = gate.shape[1]
     n_hid, width = down.shape[1], down.shape[2]
@@ -69,8 +70,14 @@
         pltpu.make_async_copy(tokens_hbm, tok, local_sem.at[0]),
         pltpu.make_async_copy(gate_hbm, gate.at[fs], local_sem.at[1]),
         pltpu.make_async_copy(up_hbm, up.at[fs], local_sem.at[2]),
-        pltpu.make_async_copy(down_hbm, down.at[fs], local_sem.at[3]),
     ]
+    for j in range(cuts):
+        cols = pl.ds(j * width, width)
+        loads.append(
+            pltpu.make_async_copy(
+                down_hbm.at[:, cols], down.at[fs * cuts + j], local_sem.at[3 + j]
+            )
+        )
     for load in loads:
         load.start()
     pl.semaphore_wait(barrier, 2 + n_tp - 1)
@@ -81,7 +88,9 @@
             if h == half:
                 return ref.at[b, pl.ds(way * (rows_in // 2), rows_in // 2)]
             return ref.at[b]
-        return down.at[b, pl.ds((c - 2) * (n_hid // 2), n_hid // 2)]
+        if h == half:
+            return down.at[b * cuts + c - 2, pl.ds(way * (n_hid // 2), n_hid // 2)]
+        return down.at[b * cuts + c - 2]
 
     def ring_copy(c, way, h, b, first=False):
         dst = view(c, b, h, way)
@@ -143,7 +152,8 @@
     loads[1].wait()
     loads[2].wait()
     accumulate(fs, "first")
-    loads[3].wait()
+    for load in loads[3:]:
+        load.wait()
 
     for h in range(1, half + 1):
         for c in (0, 1):
@@ -152,9 +162,9 @@
                 if h < half:
                     send(c, way, h + 1)
         if h == half - 1:
-            for c in (2, 3):
+            for j in range(cuts):
                 for way in (0, 1):
-                    send(c, way, 1)
+                    send(2 + j, way, 1)
         if h < half:
             accumulate(block_of[0, h], "mid")
             accumulate(block_of[1, h], "mid")
@@ -217,24 +227,20 @@
                 ).astype(jnp.bfloat16)
                 far_copy(b, x_to, x, k, q).start()
 
-    multiply(fs)
-    pending = [fs]
+    ready = [fs * cuts + j for j in range(cuts)]
     for h in range(1, half + 1):
-        for c in (2, 3):
+        for j in range(cuts):
             for way in (0, 1):
-                if h < half or way == c - 2:
-                    arrive(c, way, h)
-                if h < half - 1 or (h == half - 1 and way == c - 2):
-                    send(c, way, h + 1)
-            if c == 2:
-                for b in pending:
-                    reduce(b)
-                pending = []
-        for way in (0, 1) if h < half else (0,):
-            multiply(block_of[way, h])
-            pending.append(block_of[way, h])
-    for b in pending:
-        reduce(b)
+                arrive(2 + j, way, h)
+                if h < half:
+                    send(2 + j, way, h + 1)
+            for way in (0, 1) if h < half else (0,):
+                ready.append(block_of[way, h] * cuts + j)
+            for b in ready:
+                multiply(b)
+            for b in ready:
+                reduce(b)
+            ready = []
 
     @pl.loop(0, PIECES)
     def _(q):
@@ -298,8 +304,9 @@
 def body(n, n_tp, tokens, norm_gain, gate_weight, up_weight, down_weight, out_gain):
     n_tok, d_model = tokens.shape
     rows_in, n_hid = gate_weight.shape
-    width = down_weight.shape[1]
-    half, nx, nb = n // 2, n_tp // 2, n // n_tp
+    cuts = max(down_weight.shape[1] // 128, 1)
+    width = down_weight.shape[1] // cuts
+    half, nx, nb = n // 2, n_tp // 2, n * cuts // n_tp
     piece = n_tok // PIECES
     bf16, f32 = jnp.bfloat16, jnp.float32
     dma = pltpu.SemaphoreType.DMA
@@ -315,19 +322,19 @@
             pltpu.VMEM((n, n_tok, rows_in), bf16),
             pltpu.VMEM((n, rows_in, n_hid), bf16),
             pltpu.VMEM((n, rows_in, n_hid), bf16),
-            pltpu.VMEM((n, n_hid, width), bf16),
+            pltpu.VMEM((n * cuts, n_hid, width), bf16),
             pltpu.VMEM((n_tok, n_hid), f32),
             pltpu.VMEM((n_tok, n_hid), f32),
             pltpu.VMEM((n_tok, n_hid), bf16),
-            pltpu.VMEM((n, n_tok, width), bf16),
+            pltpu.VMEM((n * cuts, n_tok, width), bf16),
             pltpu.VMEM((nx * nb, n_tok, width), bf16),
             pltpu.VMEM((nx, nb, n_tok, width), bf16),
             pltpu.VMEM((nb, n_tok, width), f32),
             pltpu.VMEM((PIECES, 8, piece), f32),
             pltpu.VMEM((n_tp, PIECES, 8, piece), f32),
-            dma((4,)),
-            dma((2, half, 4)),
-            dma((2, half, 4)),
+            dma((3 + cuts,)),
+            dma((2, half, 2 + cuts)),
+            dma((2, half, 2 + cuts)),
             dma((nx * nb, PIECES)),
             dma((nx * nb, PIECES)),
             dma((nx * nb, PIECES)),

time: 151 us -> 143 us (0.947)
  Pallas kernels: 149 us -> 141 us
    pallas_call x1, Pallas kernels: 149 us -> 141 us  [body(): pl.pallas_call(functools.partial(kernel, n, n_tp), out_shape=jax.ShapeDty...]
where the time goes in v2:
time: 143 us
  Pallas kernels  141 us (99%)
  local copies, waits for them, and re-layouts  2.26 us (2%)
    pallas_call x1, Pallas kernels, body(): pl.pallas_call(functools.partial(kernel, n, n_tp), out_shape=jax.ShapeDty...  141 us

profile of v2, /device:TPU:0, one launch (start us, length us, event | category | flops | bytes accessed | tf_op | source)
XLA Modules:
  0.0 143.2 jit_solution(4063185658259036058)
XLA Ops:
  0.0 140.9 %ffn_ring.1 = bf16[1024,512]{1,0:T(8,128)(2,1)} custom-call(bf16[1024,2048]{1,0:T(8,128)(2,1)} %tokens_hbm.1, f32[1,2048]{1,0:T(1,128)} %bitcast.2, bf16[256,1024]{1,0:T(8,128)(2,1)} %gate_hbm.1, bf16[256,1024]{1,0:T(8,128)(2,1)} %up_hbm.1, bf16[1024,256]{1,0:T(8,128)(2,1)} %down_hbm.1, f32[1,512]{1,0:T(1,128)} %bitcast.3), custom_call_target="tpu_custom_call" | custom-call | tf_op jit(solution)/shard_map/ffn_ring/pallas_call | solution.py:315
  140.9 2.3 %copy.8 = bf16[1024,512]{1,0:T(8,128)(2,1)} copy(bf16[1024,512]{1,0:T(8,128)(2,1)} %ffn_ring.1) | data formatting | bytes 2097152
